TPU v7x, 1024 devices: a whole 4x8x16 slice. The times are simulated.
1024 devices in a mesh: ep: 32 (over z, core), tp: 32 (over y, x).
Axes of the slice: x: 4, y: 8, z: 16, core: 2. Of those that a mesh axis runs over, the one named last changes fastest.
Arguments:
- tokens: bfloat16 [2048, 4096], P('ep', 'tp'), may hold values from -600 to 600
- in_gain: float32 [4096], P('tp'), may hold values from 0.1 to 1.9
- out_gain: float32 [4096], P('tp'), may hold values from 0.1 to 1.9
- routes: int32 [2048, 4], replicated, may hold values from 0 to 127, as said below
- route_weights: float32 [2048, 4], replicated, may hold values from 0.05 to 1
- w_gate: bfloat16 [128, 4096, 1024], P('ep', 'tp'), may hold values from -0.09375 to 0.09375
- w_up: bfloat16 [128, 4096, 1024], P('ep', 'tp'), may hold values from -0.09375 to 0.09375
- w_down: bfloat16 [128, 1024, 4096], P('ep', None, 'tp'), may hold values from -0.375 to 0.375
Outputs:
- result: bfloat16 [2048, 4096], P('ep', 'tp')
Inputs may be any that keep to these rules, and one draw needn't show every extreme that they name: `routes`: each row names 4 different experts, all in one group of 8 consecutive numbers. In the rows of one index of ep (aligned blocks of 64 rows) no expert is named by more than 4 rows, and some expert by exactly 4.
All inputs are finite; a program needn't handle non-finite values.
Results may differ from a plain program's by a relative error of at most 0.025.
Values may be sent and summed in bfloat16 or wider, within the bound.
No kernel may reach another device: no remote copies, remote signals or barrier semaphores. Data moves between devices by JAX's collectives and lax.ppermute only.
A program may use at most 32 MiB of HBM per device.

v0:
```python
import jax
import jax.numpy as jnp
from jax import lax
from jax.sharding import PartitionSpec as P

D = 4096


EPS = 1e-06


def split_up(value, dim, size):
    before, after = (value.shape[:dim], value.shape[dim + 1 :])
    return jnp.moveaxis(value.reshape(*before, size, -1, *after), dim, 0)


def sum_at_owner(value, axis, dim):
    size = lax.axis_size(axis)
    tiles = lax.all_to_all(split_up(value, dim, size), axis, 0, 0, tiled=True)
    return jnp.sum(tiles.astype(jnp.float32), axis=0)


def side_by_side(arrays, axis, dim, along):
    ends, at = ([], 0)
    for a in arrays[:-1]:
        at += a.shape[along]
        ends.append(at)
    both = jnp.concatenate(arrays, axis=along)
    return tuple(jnp.split(sum_at_owner(both, axis, dim), ends, axis=along))


def joined_along(tiles, dim):
    tiles = jnp.moveaxis(tiles, 0, dim)
    dims = tiles.shape
    return tiles.reshape(*dims[:dim], dims[dim] * dims[dim + 1], *dims[dim + 2 :])


def from_everyone(value, axis):
    size = lax.axis_size(axis)
    return lax.all_to_all(
        jnp.broadcast_to(value[None], (size, *value.shape)), axis, 0, 0, tiled=True
    )


def gather_directly(value, axis, dim):
    return joined_along(from_everyone(value, axis), dim)


def taken_together(value, axis):
    return from_everyone(value, axis).sum(axis=0)


def run_experts(slot_rows, w_gate, w_up, w_down):
    gate_part = jnp.einsum(
        "secd,edf->secf", slot_rows, w_gate, preferred_element_type=jnp.float32
    ).astype(jnp.bfloat16)
    up_part = jnp.einsum(
        "secd,edf->secf", slot_rows, w_up, preferred_element_type=jnp.float32
    ).astype(jnp.bfloat16)
    gate_share, up_share = side_by_side((gate_part, up_part), "tp", 3, 0)
    active_share = (jax.nn.silu(gate_share) * up_share).astype(jnp.bfloat16)
    active = gather_directly(active_share, "tp", 3)
    return jnp.einsum("secf,efd->secd", active, w_down, preferred_element_type=jnp.float32).astype(
        jnp.bfloat16
    )


def on_device(tokens, in_gain, out_gain, routes, route_weights, w_gate, w_up, w_down):
    tok_rows, local_width = tokens.shape
    top_count = routes.shape[1]
    local_experts = w_gate.shape[0]
    groups_ep = lax.axis_size("ep")
    experts = local_experts * groups_ep
    capacity = max(2, 2 * tok_rows * top_count // experts)
    values = tokens.astype(jnp.float32)
    sum_squares = taken_together(jnp.sum(values * values, axis=1), "tp")
    normed = (values * lax.rsqrt(sum_squares / D + EPS)[:, None] * in_gain).astype(jnp.bfloat16)
    row_start = lax.axis_index("ep") * tok_rows
    my_routes = lax.dynamic_slice_in_dim(routes, row_start, tok_rows, 0)
    my_weights = lax.dynamic_slice_in_dim(route_weights, row_start, tok_rows, 0)
    flat_ids = my_routes.reshape(-1)
    matches = (flat_ids[:, None] == jnp.arange(experts, dtype=jnp.int32)[None, :]).astype(jnp.int32)
    slot_rank = jnp.sum((jnp.cumsum(matches, axis=0) - matches) * matches, axis=1)
    position = flat_ids * capacity + slot_rank
    dispatch_table = jnp.any(
        position.reshape(tok_rows, top_count, 1)
        == jnp.arange(experts * capacity, dtype=jnp.int32)[None, None, :],
        axis=1,
    )
    outgoing = jnp.einsum(
        "ts,td->sd", dispatch_table.astype(jnp.bfloat16), normed, preferred_element_type=jnp.float32
    ).astype(jnp.bfloat16)
    outgoing = outgoing.reshape(groups_ep, local_experts, capacity, local_width)
    answers = run_experts(
        lax.all_to_all(outgoing, "ep", split_axis=0, concat_axis=0, tiled=True),
        w_gate,
        w_up,
        w_down,
    )
    returned = lax.all_to_all(answers, "ep", split_axis=0, concat_axis=0, tiled=True)
    flat_out = returned.reshape(experts * capacity, local_width)
    picked = flat_out[position].reshape(tok_rows, top_count, local_width)
    combined = jnp.sum(my_weights[:, :, None] * picked.astype(jnp.float32), axis=1)
    out_squares = taken_together(jnp.sum(combined * combined, axis=1), "tp")
    return (combined * lax.rsqrt(out_squares / D + EPS)[:, None] * out_gain).astype(jnp.bfloat16)


def solution(mesh):
    placed = (
        P("ep", "tp"),
        P("tp"),
        P("tp"),
        P(),
        P(),
        P("ep", "tp", None),
        P("ep", "tp", None),
        P("ep", None, "tp"),
    )
    return jax.shard_map(
        on_device, mesh=mesh, in_specs=placed, out_specs=P("ep", "tp"), check_vma=False
    )
```

profile of v0, /device:TPU:2, one launch (start us, length us, event | category | flops | bytes accessed | tf_op | source)
XLA Modules:
  0.0 237.7 jit_solution(17261330611910819883)
XLA Ops:
  0.0 0.0 copy-start
  0.0 1.0 fusion.16
  1.0 0.6 broadcast_in_dim.6
  1.6 16.6 %all-to-all-start = ((f32[32,1,64]{2,1,0:T(1,128)}), f32[32,1,64]{2,1,0:T(1,128)S(1)}, u32[]{:S(2)}, u32[]{:S(2)}) async-start(f32[32,1,64]{2,1,0:T(1,128)} %broadcast_in_dim.6), calls=%async_computation | async-start | bytes 32768 | tf_op jit(solution)/shard_map/all_to_all | solution.py:40
  18.3 0.8 constant_dynamic-slice_fusion
  19.0 0.1 copy.63
  19.1 0.1 eq.42
  19.2 0.1 eq.38
  19.3 0.1 copy.46
  19.4 0.2 fusion.8
  19.7 0.2 fusion.11
  19.9 0.1 reduce_sum.68
  20.1 0.1 copy.48
  20.1 0.1 fusion.6
  20.3 6.6 %all-to-all-done = f32[32,1,64]{2,1,0:T(1,128)S(1)} async-done(((f32[32,1,64]{2,1,0:T(1,128)}), f32[32,1,64]{2,1,0:T(1,128)S(1)}, u32[]{:S(2)}, u32[]{:S(2)}) %all-to-all-start) | async-done | bytes 8224 | tf_op jit(solution)/shard_map/all_to_all | solution.py:40
  26.9 1.0 convolution_convert_fusion.3
  27.9 29.6 %all_to_all.32 = bf16[32,4,4,128]{3,2,1,0:T(4,128)(2,1)S(1)} all-to-all(bf16[32,4,4,128]{3,2,1,0:T(4,128)(2,1)S(1)} %bitcast.67), channel_id=1, replica_groups=mesh['ep'=32,'tp'=32] {'ep'}, dimensions={0} | all-to-all | bytes 262144 | tf_op jit(solution)/shard_map/all_to_all | solution.py:95
  57.5 0.4 fusion
  57.9 0.0 copy-done.1
  58.0 0.4 fusion.1
  58.4 0.2 pad_maximum_fusion
  58.6 3.2 %copy.52 = bf16[64,4,4,1024]{0,3,2,1:T(8,128)(2,1)} copy(bf16[64,4,4,1024]{3,0,2,1:T(8,128)(2,1)S(1)} %pad_maximum_fusion) | data formatting | bytes 4194304 | tf_op jit(solution)/shard_map/concatenate | solution.py:28
  61.8 5.5 %copy.71 = bf16[32,64,4,4,32]{1,4,3,2,0:T(8,128)(2,1)} copy(bf16[32,64,4,4,32]{1,4,0,3,2:T(8,128)(2,1)} %bitcast.62) | data formatting | bytes 4194304 | tf_op jit(solution)/shard_map/transpose | solution.py:14
  67.3 6.8 %reshape.111 = bf16[32,2,16384]{2,1,0:T(2,128)(2,1)S(1)} reshape(bf16[32,4,4,32,64]{4,3,2,1,0:T(8,128)(2,1)} %bitcast.63) | data formatting | bytes 4194304
  74.1 54.8 %all_to_all.33 = bf16[32,2,16384]{2,1,0:T(2,128)(2,1)} all-to-all(bf16[32,2,16384]{2,1,0:T(2,128)(2,1)S(1)} %reshape.111), channel_id=1, replica_groups=mesh['ep'=32,'tp'=32] {'tp'}, dimensions={0} | all-to-all | bytes 4194304 | tf_op jit(solution)/shard_map/all_to_all | solution.py:19
  128.9 7.9 %reshape.112 = bf16[32,4,4,32,64]{4,3,2,1,0:T(8,128)(2,1)} reshape(bf16[32,2,16384]{2,1,0:T(2,128)(2,1)} %all_to_all.33) | data formatting | bytes 4194304
  136.9 3.0 %convert_reduce_fusion = f32[64,4,4,32]{0,3,2,1:T(8,128)S(1)} fusion(bf16[32,4,4,32,64]{4,3,2,1,0:T(8,128)(2,1)} %reshape.112), kind=kLoop, calls=%fused_computation.1 | loop fusion | flops 2064384 | bytes 2228224 | tf_op jit(solution)/shard_map/reduce_sum | solution.py:20
  139.9 0.1 fusion.7
  140.1 0.1 copy.55
  140.2 3.0 %broadcast_bitcast_fusion = bf16[32,4,4,32,32]{4,3,2,1,0:T(8,128)(2,1)} fusion(bf16[32,4,4,32]{3,0,2,1:T(8,128)(2,1)S(1)} %copy.55), kind=kLoop, calls=%fused_computation.50 | loop fusion | bytes 1081344
  143.2 6.7 %reshape.113 = bf16[32,2,8192]{2,1,0:T(2,128)(2,1)S(1)} reshape(bf16[32,4,4,32,32]{4,3,2,1,0:T(8,128)(2,1)} %broadcast_bitcast_fusion) | data formatting | bytes 2097152
  149.8 32.1 %all_to_all.34 = bf16[32,2,8192]{2,1,0:T(2,128)(2,1)S(1)} all-to-all(bf16[32,2,8192]{2,1,0:T(2,128)(2,1)S(1)} %reshape.113), channel_id=1, replica_groups=mesh['ep'=32,'tp'=32] {'tp'}, dimensions={0} | all-to-all | bytes 2097152 | tf_op jit(solution)/shard_map/all_to_all | solution.py:40
  181.9 3.5 %reshape.114 = bf16[32,4,4,32,32]{4,3,2,1,0:T(8,128)(2,1)} reshape(bf16[32,2,8192]{2,1,0:T(2,128)(2,1)S(1)} %all_to_all.34) | data formatting | bytes 2097152
  185.5 3.1 %bitcast_bitcast_fusion = bf16[32,4,4,32,32]{4,0,2,1,3:T(8,128)(2,1)S(1)} fusion(bf16[32,4,4,32,32]{4,3,2,1,0:T(8,128)(2,1)} %reshape.114), kind=kLoop, calls=%fused_computation.48 | loop fusion | bytes 2097152 | tf_op jit(solution)/shard_map/transpose | solution.py:33
  188.6 4.6 %copy.56 = bf16[32,4,4,32,32]{4,3,0,2,1:T(8,128)(2,1)} copy(bf16[32,4,4,32,32]{4,0,2,1,3:T(8,128)(2,1)S(1)} %bitcast_bitcast_fusion) | data formatting | bytes 2097152 | tf_op jit(solution)/shard_map/transpose | solution.py:33
  193.3 6.3 %reshape.97 = bf16[32,4,4,1024]{3,0,2,1:T(8,128)(2,1)S(1)} reshape(bf16[32,4,4,32,32]{4,3,0,2,1:T(8,128)(2,1)} %copy.56) | data formatting | bytes 2097152 | tf_op jit(solution)/shard_map/reshape | solution.py:35
  199.5 0.4 fusion.2
  199.9 0.7 copy.57
  200.7 4.1 %all-to-all-start.4 = ((bf16[32,4,4,128]{3,2,1,0:T(4,128)(2,1)}), bf16[32,4,4,128]{3,2,1,0:T(4,128)(2,1)S(1)}, u32[]{:S(2)}, u32[]{:S(2)}) async-start(bf16[32,4,4,128]{3,2,1,0:T(4,128)(2,1)} %copy.57), calls=%async_computation.4 | async-start | bytes 262144 | tf_op jit(solution)/shard_map/all_to_all | solution.py:100
  204.8 0.1 mul.89
  204.9 0.8 constant_dynamic-slice_fusion.1
  205.6 0.1 copy.44
  205.8 16.2 %all-to-all-done.4 = bf16[32,4,4,128]{3,2,1,0:T(4,128)(2,1)S(1)} async-done(((bf16[32,4,4,128]{3,2,1,0:T(4,128)(2,1)}), bf16[32,4,4,128]{3,2,1,0:T(4,128)(2,1)S(1)}, u32[]{:S(2)}, u32[]{:S(2)}) %all-to-all-start.4) | async-done | bytes 131104 | tf_op jit(solution)/shard_map/all_to_all | solution.py:100
  222.0 0.9 gather_fusion
  222.8 0.1 fusion.9
  223.0 0.1 multiply_reduce_fusion
  223.1 13.9 %all_to_all.35 = f32[32,1,64]{2,1,0:T(1,128)S(1)} all-to-all(f32[32,1,64]{2,1,0:T(1,128)S(1)} %broadcast_in_dim.8), channel_id=1, replica_groups=mesh['ep'=32,'tp'=32] {'tp'}, dimensions={0} | all-to-all | bytes 16384 | tf_op jit(solution)/shard_map/all_to_all | solution.py:40
  237.1 0.7 multiply_convert_fusion
  (20 shorter events, 0.2 us)
Async XLA Ops:
  0.0 57.5 %copy-start = (bf16[4,128,1024]{2,1,0:T(8,128)(2,1)S(1)}, bf16[4,128,1024]{2,1,0:T(8,128)(2,1)}, u32[]{:S(2)}) copy-start(bf16[4,128,1024]{2,1,0:T(8,128)(2,1)} %param.13) | copy-start | bytes 3145732
  0.0 57.9 %copy-start.1 = (bf16[4,128,1024]{2,1,0:T(8,128)(2,1)S(1)}, bf16[4,128,1024]{2,1,0:T(8,128)(2,1)}, u32[]{:S(2)}) copy-start(bf16[4,128,1024]{2,1,0:T(8,128)(2,1)} %param.14) | copy-start | bytes 3145732
  1.6 25.2 %all-to-all-start = ((f32[32,1,64]{2,1,0:T(1,128)}), f32[32,1,64]{2,1,0:T(1,128)S(1)}, u32[]{:S(2)}, u32[]{:S(2)}) async-start(f32[32,1,64]{2,1,0:T(1,128)} %broadcast_in_dim.6), calls=%async_computation | async-start | bytes 32768 | tf_op jit(solution)/shard_map/all_to_all | solution.py:40
  193.2 6.3 %copy-start.2 = (bf16[4,1024,128]{2,1,0:T(8,128)(2,1)S(1)}, bf16[4,1024,128]{2,1,0:T(8,128)(2,1)}, u32[]{:S(2)}) copy-start(bf16[4,1024,128]{2,1,0:T(8,128)(2,1)} %param.15) | copy-start | bytes 3145732
  193.2 43.8 %copy-start.3 = (f32[128]{0:T(128)S(1)}, f32[128]{0:T(128)}, u32[]{:S(2)}) copy-start(f32[128]{0:T(128)} %param.10) | copy-start | bytes 1540
  200.7 21.3 %all-to-all-start.4 = ((bf16[32,4,4,128]{3,2,1,0:T(4,128)(2,1)}), bf16[32,4,4,128]{3,2,1,0:T(4,128)(2,1)S(1)}, u32[]{:S(2)}, u32[]{:S(2)}) async-start(bf16[32,4,4,128]{3,2,1,0:T(4,128)(2,1)} %copy.57), calls=%async_computation.4 | async-start | bytes 262144 | tf_op jit(solution)/shard_map/all_to_all | solution.py:100
where the time goes:
time: 239 us; the launch traced here: 238 us
  blocking collectives  130 us (54%)
  local copies, waits for them, and re-layouts  55.3 us (23%)
  waiting for transfers between devices  22.8 us (10%)
  starting transfers between devices  20.7 us (9%)
  other arithmetic  5.97 us (2%)
    all_to_all x1, blocking collectives, sum_at_owner(): tiles = lax.all_to_all(split_up(value, dim, size), axis, 0, 0, tiled=True)  54.8 us
    all_to_all x2, blocking collectives, from_everyone(): lax.all_to_all(jnp.broadcast_to(value[None], (size, *value.shape)), axis,...  46 us
    all_to_all x1, blocking collectives, on_device(): lax.all_to_all(outgoing, 'ep', split_axis=0, concat_axis=0, tiled=True)  29.6 us
    unnamed x15, local copies, waits for them, and re-layouts  28.1 us
    all_to_all x1, starting transfers between devices, from_everyone(): lax.all_to_all(jnp.broadcast_to(value[None], (size, *value.shape)), axis,...  16.6 us
    all_to_all x1, waiting for transfers between devices, on_device(): lax.all_to_all(answers, 'ep', split_axis=0, concat_axis=0, tiled=True)  16.2 us
    transpose x2, local copies, waits for them, and re-layouts, joined_along(): tiles = jnp.moveaxis(tiles, 0, dim)  7.77 us
    all_to_all x1, waiting for transfers between devices, from_everyone(): lax.all_to_all(jnp.broadcast_to(value[None], (size, *value.shape)), axis,...  6.55 us
  transfers between devices with their start and end apart: 2, of which 2 were waited for; matrix products, arithmetic and copies ran while one was open for 1% of the time, Pallas kernels for 0%

commit v1 on v0

v1 whole, which is shorter than its diff:
```python
import jax
import jax.numpy as jnp
from jax import lax
from jax.experimental import pallas as pl
from jax.experimental.pallas import tpu as pltpu
from jax.sharding import Mesh, PartitionSpec as P

EPS = 1e-06
BF, F32 = jnp.bfloat16, jnp.float32
LANES = 128
HALF = 64
CAP = 4
GROUP = 8
PARAMS = pltpu.CompilerParams(vmem_limit_bytes=16 * 1024 * 1024)


def iota(shape, dim):
    return lax.broadcasted_iota(jnp.int32, shape, dim)


def ones_where(mask, dtype=BF):
    return jnp.where(mask, 1.0, 0.0).astype(dtype)


def earlier():
    s, t = iota((LANES, LANES), 0), iota((LANES, LANES), 1)
    return ones_where((s < t) & ((s >> 6) == (t >> 6)))


def dot(a, b):
    return jnp.dot(a, b, preferred_element_type=F32)


def dot_rows(a, b):
    return lax.dot_general(a, b, (((0,), (0,)), ((), ())), preferred_element_type=F32)


def call(kernel, outs, *args, name):
    single = not isinstance(outs, (list, tuple))
    return pl.pallas_call(
        kernel,
        out_shape=outs,
        in_specs=[pl.BlockSpec(memory_space=pltpu.VMEM)] * len(args),
        out_specs=pl.BlockSpec(memory_space=pltpu.VMEM)
        if single
        else [pl.BlockSpec(memory_space=pltpu.VMEM)] * len(outs),
        compiler_params=PARAMS,
        name=name,
    )(*args)


def shape(dims, dtype):
    return jax.ShapeDtypeStruct(dims, dtype)


def dispatch_kernel(routes_ref, tok_ref, out_ref, place_ref):
    z, c = lax.axis_index("z"), lax.axis_index("c")
    group = routes_ref[z, 0:1, :] >> 3
    chips = routes_ref.shape[0]
    member = iota((chips, LANES), 0) == group
    rank = dot(ones_where(member), earlier())
    rank = jnp.sum(jnp.where(member, rank, 0.0), axis=0, keepdims=True).astype(jnp.int32)
    mine = (iota((1, LANES), 1) >> 6) == c
    row = jnp.where(mine, group * GROUP + rank, -1)
    place = ones_where(iota((LANES, LANES), 0) == row)
    place_ref[...] = place
    tok = tok_ref[...]
    out_ref[...] = dot(place, jnp.concatenate([tok, tok], axis=0)).astype(BF)


def table_kernel(routes_ref, weights_ref, sel_ref, scale_ref):
    z, c, x = lax.axis_index("z"), lax.axis_index("c"), lax.axis_index("x")
    chips = routes_ref.shape[0]
    ids = [routes_ref[:, k, :] for k in range(CAP)]
    before = earlier()
    base = z * GROUP

    def named(expert):
        hit = ids[0] == expert
        for k in range(1, CAP):
            hit = hit | (ids[k] == expert)
        return jnp.where(hit, 1.0, 0.0)

    rows = [named(base + e) for e in range(GROUP)]
    hits = jnp.concatenate(rows, axis=0)
    anyone = rows[0]
    for e in range(1, GROUP):
        anyone = jnp.maximum(anyone, rows[e])
    rank = dot(hits.astype(BF), before)
    spot = dot(anyone.astype(BF), before) + (iota((chips, LANES), 0) * GROUP).astype(F32)
    spots = jnp.concatenate([spot] * GROUP, axis=0)
    block = iota((LANES, LANES), 1) >> 6
    lane = iota((LANES, LANES), 1).astype(F32)
    live = (hits > 0.0) & (block == c)
    for q in range(CAP):
        at = jnp.sum(jnp.where(live & (rank == q), spots + 1.0, 0.0), axis=1, keepdims=True) - 1.0
        sel_ref[q] = ones_where(lane == at)
    own = base + c * CAP + x
    own_hit = named(own)
    own_rank = dot(own_hit.astype(BF), before)
    weight = jnp.zeros((chips, LANES), F32)
    for k in range(CAP):
        weight = weight + jnp.where(ids[k] == own, weights_ref[:, k, :], 0.0)
    small_block = iota((chips, LANES), 1) >> 6
    for core in range(2):
        for q in range(CAP):
            at = (own_hit > 0.0) & (own_rank == q) & (small_block == core)
            value = jnp.sum(jnp.where(at, weight, 0.0), axis=1, keepdims=True)
            start = (core * CAP + q) * chips
            scale_ref[start : start + chips, :] = jnp.broadcast_to(value, (chips, LANES))


def select_kernel(recv_ref, sel_ref, gain_ref, out_ref):
    recv = recv_ref[...]
    for q in range(CAP):
        picked = dot(sel_ref[q], recv).astype(BF)
        for e in range(GROUP):
            out_ref[e, q * 16 : (q + 1) * 16, :] = picked[e * 16 : (e + 1) * 16]
    gain = gain_ref[...]
    high = gain.astype(BF)
    rest = gain - high.astype(F32)
    middle = rest.astype(BF)
    low = (rest - middle.astype(F32)).astype(BF)
    row = iota((8, LANES), 0)
    tail = jnp.where(
        row == 0,
        high.astype(F32),
        jnp.where(row == 1, middle.astype(F32), jnp.where(row == 2, low.astype(F32), 0.0)),
    ).astype(BF)
    for e in range(GROUP):
        out_ref[e, 64:72, :] = tail


def gate_up_kernel(rows_ref, gate_ref, up_ref, out_ref):
    squares = jnp.zeros((LANES, 1), F32)
    parts = []
    for x in range(4):
        raw = jnp.concatenate([rows_ref[x, 0:64, :], rows_ref[4 + x, 0:64, :]], axis=0).astype(F32)
        tail = rows_ref[x, 64:72, :].astype(F32)
        gain = tail[0:1] + tail[1:2] + tail[2:3]
        squares = squares + jnp.sum(raw * raw, axis=1, keepdims=True)
        parts.append((raw * gain).astype(BF))
    lhs = jnp.concatenate(parts, axis=1)
    hidden = gate_ref.shape[1]
    out_ref[:, 0:hidden] = dot(lhs, gate_ref[...]).astype(BF)
    out_ref[:, hidden : 2 * hidden] = dot(lhs, up_ref[...]).astype(BF)
    high = squares.astype(BF).astype(F32)
    lane = iota((LANES, LANES), 1)
    out_ref[:, 2 * hidden :] = jnp.where(lane < HALF, high, squares - high).astype(BF)


def act_kernel(width, parts_ref, out_ref):
    total = parts_ref[0].astype(F32)
    for y in range(1, parts_ref.shape[0]):
        total = total + parts_ref[y].astype(F32)
    hidden = out_ref.shape[2]
    squares = total[:, 2 * hidden : 2 * hidden + 1] + total[:, 2 * hidden + HALF : 2 * hidden + HALF + 1]
    scale = lax.rsqrt(squares / width + EPS)
    gate = total[:, 0:hidden] * scale
    up = total[:, hidden : 2 * hidden] * scale
    act = (gate / (1.0 + jnp.exp(-gate)) * up).astype(BF)
    for y in range(out_ref.shape[0]):
        out_ref[y] = act


def down_kernel(act_ref, down_ref, scale_ref, out_ref):
    act = act_ref[...]
    scale = scale_ref[...]
    for x in range(4):
        out = (dot(act, down_ref[x]) * scale).astype(BF)
        out_ref[x] = out[0:64]
        out_ref[4 + x] = out[64:128]


def combine_kernel(parts_ref, sel_ref, out_ref):
    total = jnp.zeros((LANES, LANES), F32)
    for q in range(CAP):
        rows = jnp.concatenate(
            [parts_ref[e, q * 16 : (q + 1) * 16, :] for e in range(GROUP)], axis=0
        )
        total = total + dot_rows(sel_ref[q], rows)
    out_ref[...] = total.astype(BF)


def place_kernel(ret_ref, place_ref, comb_ref, squares_ref):
    full = dot_rows(place_ref[...], ret_ref[...])
    comb_ref[...] = full[0:HALF] + full[HALF:LANES]
    squares = jnp.sum(full * full, axis=1, keepdims=True)
    flat = jnp.transpose(jnp.broadcast_to(squares, (LANES, LANES)))[0:1, :]
    for i in range(squares_ref.shape[0]):
        squares_ref[i] = flat


def norm_kernel(width, squares_ref, comb_ref, gain_ref, out_ref):
    total = squares_ref[0]
    for i in range(1, squares_ref.shape[0]):
        total = total + squares_ref[i]
    column = jnp.transpose(jnp.broadcast_to(total, (LANES, LANES)))
    column = column[0:HALF] + column[HALF:LANES]
    out_ref[...] = (comb_ref[...] * lax.rsqrt(column / width + EPS) * gain_ref[...]).astype(BF)


def exchange(value, axes):
    return lax.all_to_all(value, axes, 0, 0, tiled=True)


def on_device(tokens, in_gain, out_gain, routes, route_weights, w_gate, w_up, w_down):
    chips, ys, xs = lax.axis_size("z"), lax.axis_size("y"), lax.axis_size("x")
    local = tokens.shape[1]
    width = float(local * ys * xs)
    hidden = w_gate.shape[2]
    routes = jnp.transpose(routes.reshape(chips, LANES, CAP), (0, 2, 1))
    weights = jnp.transpose(route_weights.reshape(chips, LANES, CAP), (0, 2, 1))

    gate_rows = exchange(w_gate, "x").reshape(xs * local, hidden)
    up_rows = exchange(w_up, "x").reshape(xs * local, hidden)
    outgoing, place = call(
        dispatch_kernel,
        [shape((LANES, LANES), BF), shape((LANES, LANES), BF)],
        routes,
        tokens,
        name="dispatch",
    )
    sel, scale = call(
        table_kernel,
        [shape((CAP, LANES, LANES), BF), shape((LANES, LANES), F32)],
        routes,
        weights,
        name="tables",
    )
    arrived = exchange(outgoing.reshape(chips, GROUP, local), "z").reshape(LANES, local)
    slots = call(
        select_kernel,
        shape((GROUP, 72, LANES), BF),
        arrived,
        sel,
        in_gain.reshape(1, local),
        name="select",
    )
    slots = exchange(slots, ("c", "x"))
    parts = call(
        gate_up_kernel,
        shape((LANES, 2 * hidden + LANES), BF),
        slots,
        gate_rows,
        up_rows,
        name="gate_up",
    )
    down_rows = exchange(w_down, "x")
    parts = exchange(parts.reshape(ys, LANES // ys, 2 * hidden + LANES), "y")
    act = call(
        lambda *refs: act_kernel(width, *refs),
        shape((ys, LANES // ys, hidden), BF),
        parts,
        name="act",
    )
    act = exchange(act, "y").reshape(LANES, hidden)
    answers = call(
        down_kernel, shape((GROUP, 64, LANES), BF), act, down_rows, scale, name="down"
    )
    answers = exchange(answers, ("c", "x"))
    mixed = call(combine_kernel, shape((LANES, local), BF), answers, sel, name="combine")
    returned = exchange(mixed.reshape(chips, GROUP, local), "z").reshape(LANES, local)
    combined, squares = call(
        place_kernel,
        [shape((HALF, local), F32), shape((ys * xs, 1, LANES), F32)],
        returned,
        place,
        name="place",
    )
    squares = exchange(squares, ("y", "x"))
    return call(
        lambda *refs: norm_kernel(width, *refs),
        shape((HALF, local), BF),
        squares,
        combined,
        out_gain.reshape(1, local),
        name="norm",
    )


def solution(mesh):
    fine = Mesh(
        mesh.devices.reshape(mesh.shape["ep"] // 2, 2, mesh.shape["tp"] // 4, 4),
        ("z", "c", "y", "x"),
    )
    ep, tp = ("z", "c"), ("y", "x")
    placed = (
        P(ep, tp),
        P(tp),
        P(tp),
        P(),
        P(),
        P(ep, tp, None),
        P(ep, tp, None),
        P(ep, None, tp),
    )
    return jax.shard_map(
        on_device, mesh=fine, in_specs=placed, out_specs=P(ep, tp), check_vma=False
    )
```

time: 239 us -> 173 us (0.72)
  local copies, waits for them, and re-layouts: 55.3 us -> 2.8 us
  blocking collectives: 130 us -> 119 us
  other arithmetic: 5.97 us -> 0 us
  Pallas kernels: 0 us -> 3.94 us
  starting transfers between devices: 20.7 us -> 23.9 us
    unnamed x15 -> x14, local copies, waits for them, and re-layouts: 28.1 us -> 2.8 us
    transpose x3 -> x0, local copies, waits for them, and re-layouts: 13.3 us -> none  [the longest x2 7.77 us: joined_along(): tiles = jnp.moveaxis(tiles, 0, dim)]
    all_to_all x4 -> x8, blocking collectives: 130 us -> 119 us  [exchange(): return lax.all_to_all(value, axes, 0, 0, tiled=True)]
    reshape x1 -> x0, local copies, waits for them, and re-layouts: 6.25 us -> none  [joined_along(): tiles.reshape(*dims[:dim], dims[dim] * dims[dim + 1], *dims[dim + 2:])]
    reduce_sum x7 -> x0, other arithmetic: 4.49 us -> none  [the longest x1 3.04 us: sum_at_owner(): return jnp.sum(tiles.astype(jnp.float32), axis=0)]
    pallas_call x0 -> x9, Pallas kernels: none -> 3.94 us  [call(): pl.pallas_call(kernel, out_shape=outs, in_specs=[pl.BlockSpec(memory_spac...]
    all_to_all x2, starting transfers between devices: 20.7 us -> 23.9 us  [exchange(): return lax.all_to_all(value, axes, 0, 0, tiled=True)]
    concatenate x1 -> x0, local copies, waits for them, and re-layouts: 3.18 us -> none  [side_by_side(): both = jnp.concatenate(arrays, axis=along)]
  transfers between devices with their start and end apart: 2 -> 2, of which waited for: 2 -> 2; matrix products, arithmetic and copies ran while one was open for 1% -> 0% of each run, Pallas kernels for 0% -> 0%
where the time goes in v1:
time: 173 us; the launch traced here: 172 us
  blocking collectives  119 us (69%)
  starting transfers between devices  23.9 us (14%)
  waiting for transfers between devices  22.5 us (13%)
  Pallas kernels  3.94 us (2%)
  local copies, waits for them, and re-layouts  2.8 us (2%)
    all_to_all x8, blocking collectives, exchange(): return lax.all_to_all(value, axes, 0, 0, tiled=True)  119 us
    all_to_all x2, starting transfers between devices, exchange(): return lax.all_to_all(value, axes, 0, 0, tiled=True)  23.9 us
    all_to_all x2, waiting for transfers between devices, exchange(): return lax.all_to_all(value, axes, 0, 0, tiled=True)  22.5 us
    pallas_call x9, Pallas kernels, call(): pl.pallas_call(kernel, out_shape=outs, in_specs=[pl.BlockSpec(memory_spac...  3.94 us
  transfers between devices with their start and end apart: 2, of which 2 were waited for; matrix products, arithmetic and copies ran while one was open for 0% of the time, Pallas kernels for 0%

profile of v1, /device:TPU:2, one launch (start us, length us, event | category | flops | bytes accessed | tf_op | source)
XLA Modules:
  0.0 171.8 jit_solution(1504400559118416083)
XLA Ops:
  0.0 0.0 copy-start
  0.0 0.8 copy-done
  0.8 0.0 copy-start.3
  0.8 0.7 copy-done.3
  1.5 0.9 dispatch.1
  2.4 0.0 copy-start.1
  2.4 0.0 copy-start.2
  2.4 19.0 %all-to-all-start = ((bf16[16,8,128]{2,1,0:T(8,128)(2,1)}), bf16[16,8,128]{2,1,0:T(8,128)(2,1)S(1)}, u32[]{:S(2)}, u32[]{:S(2)}) async-start(bf16[16,8,128]{2,1,0:T(8,128)(2,1)} %bitcast.2), calls=%async_computation | async-start | bytes 65536 | tf_op jit(solution)/shard_map/all_to_all | solution.py:204
  21.4 0.0 copy-done.1
  21.4 0.0 copy-done.2
  21.4 0.6 tables.1
  21.9 12.0 %all-to-all-done = bf16[16,8,128]{2,1,0:T(8,128)(2,1)S(1)} async-done(((bf16[16,8,128]{2,1,0:T(8,128)(2,1)}), bf16[16,8,128]{2,1,0:T(8,128)(2,1)S(1)}, u32[]{:S(2)}, u32[]{:S(2)}) %all-to-all-start) | async-done | bytes 32800 | tf_op jit(solution)/shard_map/all_to_all | solution.py:204
  33.9 0.0 copy-start.4
  33.9 0.7 copy-done.4
  34.6 0.2 select.1
  34.8 9.3 %all_to_all.50.rows_ref = bf16[8,72,128]{2,1,0:T(8,128)(2,1)S(1)} all-to-all(bf16[8,72,128]{2,1,0:T(8,128)(2,1)S(1)} %select.1), channel_id=1, replica_groups=mesh['z'=16,'c'=2,'y'=8,'x'=4] {'c','x'}, dimensions={0} | all-to-all | bytes 294912 | tf_op jit(solution)/shard_map/all_to_all | solution.py:204
  44.0 0.0 copy-start.6
  44.0 18.9 %all_to_all.51 = bf16[4,128,1024]{2,1,0:T(8,128)(2,1)S(1)} all-to-all(bf16[4,128,1024]{2,1,0:T(8,128)(2,1)} %param.13), channel_id=1, replica_groups=mesh['z'=16,'c'=2,'y'=8,'x'=4] {'x'}, dimensions={0} | all-to-all | bytes 2097152 | tf_op jit(solution)/shard_map/all_to_all | solution.py:204
  62.9 0.0 copy-done.6
  62.9 17.2 %all_to_all.52 = bf16[4,128,1024]{2,1,0:T(8,128)(2,1)S(1)} all-to-all(bf16[4,128,1024]{2,1,0:T(8,128)(2,1)S(1)} %copy-done.6), channel_id=1, replica_groups=mesh['z'=16,'c'=2,'y'=8,'x'=4] {'x'}, dimensions={0} | all-to-all | bytes 2097152 | tf_op jit(solution)/shard_map/all_to_all | solution.py:204
  80.1 0.5 gate_up.1
  80.6 23.7 %all_to_all.53.refs_0_ = bf16[8,16,2176]{2,1,0:T(8,128)(2,1)S(1)} all-to-all(bf16[8,16,2176]{2,1,0:T(8,128)(2,1)S(1)} %bitcast.18), channel_id=1, replica_groups=mesh['z'=16,'c'=2,'y'=8,'x'=4] {'y'}, dimensions={0} | all-to-all | bytes 1114112 | tf_op jit(solution)/shard_map/all_to_all | solution.py:204
  104.3 4.9 %all-to-all-start.6 = ((bf16[4,1024,128]{2,1,0:T(8,128)(2,1)}), bf16[4,1024,128]{2,1,0:T(8,128)(2,1)S(1)}, u32[]{:S(2)}, u32[]{:S(2)}) async-start(bf16[4,1024,128]{2,1,0:T(8,128)(2,1)} %param.15), calls=%async_computation.6 | async-start | bytes 2097152 | tf_op jit(solution)/shard_map/all_to_all | solution.py:204
  109.2 0.2 act.1
  109.4 10.5 %all-to-all-done.6.down_ref = bf16[4,1024,128]{2,1,0:T(8,128)(2,1)S(1)} async-done(((bf16[4,1024,128]{2,1,0:T(8,128)(2,1)}), bf16[4,1024,128]{2,1,0:T(8,128)(2,1)S(1)}, u32[]{:S(2)}, u32[]{:S(2)}) %all-to-all-start.6) | async-done | bytes 1048608 | tf_op jit(solution)/shard_map/all_to_all | solution.py:204
  119.9 13.6 %all_to_all.54 = bf16[8,16,1024]{2,1,0:T(8,128)(2,1)S(1)} all-to-all(bf16[8,16,1024]{2,1,0:T(8,128)(2,1)S(1)} %act.1), channel_id=1, replica_groups=mesh['z'=16,'c'=2,'y'=8,'x'=4] {'y'}, dimensions={0} | all-to-all | bytes 524288 | tf_op jit(solution)/shard_map/all_to_all | solution.py:204
  133.5 0.4 down.1
  133.9 8.3 %all_to_all.55.parts_ref = bf16[8,64,128]{2,1,0:T(8,128)(2,1)S(1)} all-to-all(bf16[8,64,128]{2,1,0:T(8,128)(2,1)S(1)} %down.1), channel_id=1, replica_groups=mesh['z'=16,'c'=2,'y'=8,'x'=4] {'c','x'}, dimensions={0} | all-to-all | bytes 262144 | tf_op jit(solution)/shard_map/all_to_all | solution.py:204
  142.2 0.2 combine.1
  142.4 15.0 %all_to_all.56 = bf16[16,8,128]{2,1,0:T(8,128)(2,1)S(1)} all-to-all(bf16[16,8,128]{2,1,0:T(8,128)(2,1)S(1)} %bitcast.21), channel_id=1, replica_groups=mesh['z'=16,'c'=2,'y'=8,'x'=4] {'z'}, dimensions={0} | all-to-all | bytes 65536 | tf_op jit(solution)/shard_map/all_to_all | solution.py:204
  157.5 0.3 place.1
  157.8 12.6 %all_to_all.57.refs_0_ = f32[32,1,128]{2,1,0:T(1,128)S(1)} all-to-all(f32[32,1,128]{2,1,0:T(1,128)S(1)} %get-tuple-element.15), channel_id=1, replica_groups=mesh['z'=16,'c'=2,'y'=8,'x'=4] {'y','x'}, dimensions={0} | all-to-all | bytes 32768 | tf_op jit(solution)/shard_map/all_to_all | solution.py:204
  170.4 0.0 copy-start.5
  170.4 0.7 copy-done.5
  171.1 0.8 norm.1
Async XLA Ops:
  0.0 0.8 copy-start
  0.8 0.7 copy-start.3
  2.4 19.0 %copy-start.1 = (s32[2048,4]{0,1:T(4,128)S(1)}, s32[2048,4]{0,1:T(4,128)}, u32[]{:S(2)}) copy-start(s32[2048,4]{0,1:T(4,128)} %param.11) | copy-start | bytes 98308
  2.4 19.0 %copy-start.2 = (f32[2048,4]{0,1:T(4,128)S(1)}, f32[2048,4]{0,1:T(4,128)}, u32[]{:S(2)}) copy-start(f32[2048,4]{0,1:T(4,128)} %param.12) | copy-start | bytes 98308
  2.4 31.6 %all-to-all-start = ((bf16[16,8,128]{2,1,0:T(8,128)(2,1)}), bf16[16,8,128]{2,1,0:T(8,128)(2,1)S(1)}, u32[]{:S(2)}, u32[]{:S(2)}) async-start(bf16[16,8,128]{2,1,0:T(8,128)(2,1)} %bitcast.2), calls=%async_computation | async-start | bytes 65536 | tf_op jit(solution)/shard_map/all_to_all | solution.py:204
  33.9 0.7 copy-start.4
  44.0 18.9 %copy-start.6 = (bf16[4,128,1024]{2,1,0:T(8,128)(2,1)S(1)}, bf16[4,128,1024]{2,1,0:T(8,128)(2,1)}, u32[]{:S(2)}) copy-start(bf16[4,128,1024]{2,1,0:T(8,128)(2,1)} %param.14) | copy-start | bytes 3145732
  104.3 15.6 %all-to-all-start.6 = ((bf16[4,1024,128]{2,1,0:T(8,128)(2,1)}), bf16[4,1024,128]{2,1,0:T(8,128)(2,1)S(1)}, u32[]{:S(2)}, u32[]{:S(2)}) async-start(bf16[4,1024,128]{2,1,0:T(8,128)(2,1)} %param.15), calls=%async_computation.6 | async-start | bytes 2097152 | tf_op jit(solution)/shard_map/all_to_all | solution.py:204
  170.4 0.7 copy-start.5

commit v2 on v1

--- a/solution.py
+++ b/solution.py
@@ -35,7 +35,7 @@
     return lax.dot_general(a, b, (((0,), (0,)), ((), ())), preferred_element_type=F32)
 
 
-def call(kernel, outs, *args, name):
+def call(kernel, outs, *args):
     single = not isinstance(outs, (list, tuple))
     return pl.pallas_call(
         kernel,
@@ -45,7 +45,6 @@
         if single
         else [pl.BlockSpec(memory_space=pltpu.VMEM)] * len(outs),
         compiler_params=PARAMS,
-        name=name,
     )(*args)
 
 
@@ -68,20 +67,19 @@
     out_ref[...] = dot(place, jnp.concatenate([tok, tok], axis=0)).astype(BF)
 
 
-def table_kernel(routes_ref, weights_ref, sel_ref, scale_ref):
-    z, c, x = lax.axis_index("z"), lax.axis_index("c"), lax.axis_index("x")
+def named(ids, expert):
+    hit = ids[0] == expert
+    for k in range(1, CAP):
+        hit = hit | (ids[k] == expert)
+    return jnp.where(hit, 1.0, 0.0)
+
+
+def table_kernel(routes_ref, sel_ref):
+    z, c = lax.axis_index("z"), lax.axis_index("c")
     chips = routes_ref.shape[0]
     ids = [routes_ref[:, k, :] for k in range(CAP)]
     before = earlier()
-    base = z * GROUP
-
-    def named(expert):
-        hit = ids[0] == expert
-        for k in range(1, CAP):
-            hit = hit | (ids[k] == expert)
-        return jnp.where(hit, 1.0, 0.0)
-
-    rows = [named(base + e) for e in range(GROUP)]
+    rows = [named(ids, z * GROUP + e) for e in range(GROUP)]
     hits = jnp.concatenate(rows, axis=0)
     anyone = rows[0]
     for e in range(1, GROUP):
@@ -89,25 +87,69 @@
     rank = dot(hits.astype(BF), before)
     spot = dot(anyone.astype(BF), before) + (iota((chips, LANES), 0) * GROUP).astype(F32)
     spots = jnp.concatenate([spot] * GROUP, axis=0)
-    block = iota((LANES, LANES), 1) >> 6
     lane = iota((LANES, LANES), 1).astype(F32)
-    live = (hits > 0.0) & (block == c)
+    live = (hits > 0.0) & ((iota((LANES, LANES), 1) >> 6) == c)
     for q in range(CAP):
         at = jnp.sum(jnp.where(live & (rank == q), spots + 1.0, 0.0), axis=1, keepdims=True) - 1.0
         sel_ref[q] = ones_where(lane == at)
-    own = base + c * CAP + x
-    own_hit = named(own)
-    own_rank = dot(own_hit.astype(BF), before)
+
+
+def scale_kernel(routes_ref, weights_ref, scale_ref):
+    z, c, x = lax.axis_index("z"), lax.axis_index("c"), lax.axis_index("x")
+    chips = routes_ref.shape[0]
+    ids = [routes_ref[:, k, :] for k in range(CAP)]
+    own = z * GROUP + c * CAP + x
+    hit = named(ids, own)
+    rank = dot(hit.astype(BF), earlier())
     weight = jnp.zeros((chips, LANES), F32)
     for k in range(CAP):
         weight = weight + jnp.where(ids[k] == own, weights_ref[:, k, :], 0.0)
-    small_block = iota((chips, LANES), 1) >> 6
+    block = iota((chips, LANES), 1) >> 6
     for core in range(2):
         for q in range(CAP):
-            at = (own_hit > 0.0) & (own_rank == q) & (small_block == core)
+            at = (hit > 0.0) & (rank == q) & (block == core)
             value = jnp.sum(jnp.where(at, weight, 0.0), axis=1, keepdims=True)
             start = (core * CAP + q) * chips
             scale_ref[start : start + chips, :] = jnp.broadcast_to(value, (chips, LANES))
+
+
+def deal_kernel(*refs):
+    x = lax.axis_index("x")
+    n = lax.axis_size("x")
+    sources, outs, sems = refs[: len(refs) - 1 - n], refs[len(refs) - 1 - n : -1], refs[-1]
+    copies = []
+    for d in range(n):
+        for i, source in enumerate(sources):
+            copies.append(
+                pltpu.make_async_copy(
+                    source.at[lax.rem(x + d, n)], outs[d].at[i], sems.at[d * len(sources) + i]
+                )
+            )
+    for copy in copies:
+        copy.start()
+    for copy in copies:
+        copy.wait()
+
+
+def deal(arrays):
+    n = arrays[0].shape[0]
+    one = shape((len(arrays), *arrays[0].shape[1:]), BF)
+    return pl.pallas_call(
+        deal_kernel,
+        out_shape=[one] * n,
+        in_specs=[pl.BlockSpec(memory_space=pl.ANY)] * len(arrays),
+        out_specs=[pl.BlockSpec(memory_space=pltpu.VMEM)] * n,
+        scratch_shapes=[pltpu.SemaphoreType.DMA((n * len(arrays),))],
+        compiler_params=PARAMS,
+    )(*arrays)
+
+
+def passed(pieces, axis):
+    n = lax.axis_size(axis)
+    moved = [pieces[0]]
+    for d in range(1, n):
+        moved.append(lax.ppermute(pieces[d], axis, [(i, (i + d) % n) for i in range(n)]))
+    return moved
 
 
 def select_kernel(recv_ref, sel_ref, gain_ref, out_ref):
@@ -131,19 +173,26 @@
         out_ref[e, 64:72, :] = tail
 
 
-def gate_up_kernel(rows_ref, gate_ref, up_ref, out_ref):
+def gate_up_kernel(rows_ref, *refs):
+    *weights, out_ref = refs
+    n = len(weights)
+    x = lax.axis_index("x")
     squares = jnp.zeros((LANES, 1), F32)
-    parts = []
-    for x in range(4):
-        raw = jnp.concatenate([rows_ref[x, 0:64, :], rows_ref[4 + x, 0:64, :]], axis=0).astype(F32)
-        tail = rows_ref[x, 64:72, :].astype(F32)
+    hidden = weights[0].shape[2]
+    gate = jnp.zeros((LANES, hidden), F32)
+    up = jnp.zeros((LANES, hidden), F32)
+    for d in range(n):
+        at = lax.rem(x - d + n, n)
+        raw = jnp.concatenate([rows_ref[at, 0:64, :], rows_ref[n + at, 0:64, :]], axis=0)
+        raw = raw.astype(F32)
+        tail = rows_ref[at, 64:72, :].astype(F32)
         gain = tail[0:1] + tail[1:2] + tail[2:3]
         squares = squares + jnp.sum(raw * raw, axis=1, keepdims=True)
-        parts.append((raw * gain).astype(BF))
-    lhs = jnp.concatenate(parts, axis=1)
-    hidden = gate_ref.shape[1]
-    out_ref[:, 0:hidden] = dot(lhs, gate_ref[...]).astype(BF)
-    out_ref[:, hidden : 2 * hidden] = dot(lhs, up_ref[...]).astype(BF)
+        lhs = (raw * gain).astype(BF)
+        gate = gate + dot(lhs, weights[d][0])
+        up = up + dot(lhs, weights[d][1])
+    out_ref[:, 0:hidden] = gate.astype(BF)
+    out_ref[:, hidden : 2 * hidden] = up.astype(BF)
     high = squares.astype(BF).astype(F32)
     lane = iota((LANES, LANES), 1)
     out_ref[:, 2 * hidden :] = jnp.where(lane < HALF, high, squares - high).astype(BF)
@@ -163,13 +212,17 @@
         out_ref[y] = act
 
 
-def down_kernel(act_ref, down_ref, scale_ref, out_ref):
+def down_kernel(act_ref, scale_ref, *refs):
+    *weights, out_ref = refs
+    n = len(weights)
+    x = lax.axis_index("x")
     act = act_ref[...]
     scale = scale_ref[...]
-    for x in range(4):
-        out = (dot(act, down_ref[x]) * scale).astype(BF)
-        out_ref[x] = out[0:64]
-        out_ref[4 + x] = out[64:128]
+    for d in range(n):
+        at = lax.rem(x - d + n, n)
+        out = (dot(act, weights[d][0]) * scale).astype(BF)
+        out_ref[at] = out[0:64]
+        out_ref[n + at] = out[64:128]
 
 
 def combine_kernel(parts_ref, sel_ref, out_ref):
@@ -212,61 +265,28 @@
     routes = jnp.transpose(routes.reshape(chips, LANES, CAP), (0, 2, 1))
     weights = jnp.transpose(route_weights.reshape(chips, LANES, CAP), (0, 2, 1))
 
-    gate_rows = exchange(w_gate, "x").reshape(xs * local, hidden)
-    up_rows = exchange(w_up, "x").reshape(xs * local, hidden)
+    gate_up = passed(deal([w_gate, w_up]), "x")
     outgoing, place = call(
-        dispatch_kernel,
-        [shape((LANES, LANES), BF), shape((LANES, LANES), BF)],
-        routes,
-        tokens,
-        name="dispatch",
-    )
-    sel, scale = call(
-        table_kernel,
-        [shape((CAP, LANES, LANES), BF), shape((LANES, LANES), F32)],
-        routes,
-        weights,
-        name="tables",
-    )
+        dispatch_kernel, [shape((LANES, LANES), BF), shape((LANES, LANES), BF)], routes, tokens
+    )
+    sel = call(table_kernel, shape((CAP, LANES, LANES), BF), routes)
+    scale = call(scale_kernel, shape((LANES, LANES), F32), routes, weights)
     arrived = exchange(outgoing.reshape(chips, GROUP, local), "z").reshape(LANES, local)
     slots = call(
-        select_kernel,
-        shape((GROUP, 72, LANES), BF),
-        arrived,
-        sel,
-        in_gain.reshape(1, local),
-        name="select",
+        select_kernel, shape((GROUP, 72, LANES), BF), arrived, sel, in_gain.reshape(1, local)
     )
     slots = exchange(slots, ("c", "x"))
-    parts = call(
-        gate_up_kernel,
-        shape((LANES, 2 * hidden + LANES), BF),
-        slots,
-        gate_rows,
-        up_rows,
-        name="gate_up",
-    )
-    down_rows = exchange(w_down, "x")
+    parts = call(gate_up_kernel, shape((LANES, 2 * hidden + LANES), BF), slots, *gate_up)
+    down_rows = passed(deal([w_down]), "x")
     parts = exchange(parts.reshape(ys, LANES // ys, 2 * hidden + LANES), "y")
-    act = call(
-        lambda *refs: act_kernel(width, *refs),
-        shape((ys, LANES // ys, hidden), BF),
-        parts,
-        name="act",
-    )
+    act = call(lambda *refs: act_kernel(width, *refs), shape((ys, LANES // ys, hidden), BF), parts)
     act = exchange(act, "y").reshape(LANES, hidden)
-    answers = call(
-        down_kernel, shape((GROUP, 64, LANES), BF), act, down_rows, scale, name="down"
-    )
+    answers = call(down_kernel, shape((GROUP, 64, LANES), BF), act, scale, *down_rows)
     answers = exchange(answers, ("c", "x"))
-    mixed = call(combine_kernel, shape((LANES, local), BF), answers, sel, name="combine")
+    mixed = call(combine_kernel, shape((LANES, local), BF), answers, sel)
     returned = exchange(mixed.reshape(chips, GROUP, local), "z").reshape(LANES, local)
     combined, squares = call(
-        place_kernel,
-        [shape((HALF, local), F32), shape((ys * xs, 1, LANES), F32)],
-        returned,
-        place,
-        name="place",
+        place_kernel, [shape((HALF, local), F32), shape((ys * xs, 1, LANES), F32)], returned, place
     )
     squares = exchange(squares, ("y", "x"))
     return call(
@@ -275,7 +295,6 @@
         squares,
         combined,
         out_gain.reshape(1, local),
-        name="norm",
     )
 
 
@@ -295,6 +314,5 @@
         P(ep, tp, None),
         P(ep, None, tp),
     )
-    return jax.shard_map(
-        on_device, mesh=fine, in_specs=placed, out_specs=P(ep, tp), check_vma=False
-    )
+
+    return jax.shard_map(on_device, mesh=fine, in_specs=placed, out_specs=P(ep, tp), check_vma=False)

time: 173 us -> 150 us (0.87)
  blocking collectives: 119 us -> 76.2 us
  starting transfers between devices: 23.9 us -> 42.3 us
  Pallas kernels: 3.94 us -> 6.28 us
  waiting for transfers between devices: 22.5 us -> 20.5 us
    all_to_all x8 -> x5, blocking collectives: 119 us -> 76.2 us  [exchange(): return lax.all_to_all(value, axes, 0, 0, tiled=True)]
    ppermute x0 -> x6, starting transfers between devices: none -> 30.5 us  [passed(): lax.ppermute(pieces[d], axis, [(i, (i + d) % n) for i in range(n)])]
    all_to_all x2, starting transfers between devices: 23.9 us -> 11.8 us  [exchange(): return lax.all_to_all(value, axes, 0, 0, tiled=True)]
    all_to_all x2, waiting for transfers between devices: 22.5 us -> 12.1 us  [exchange(): return lax.all_to_all(value, axes, 0, 0, tiled=True)]
    ppermute x0 -> x6, waiting for transfers between devices: none -> 8.4 us  [passed(): lax.ppermute(pieces[d], axis, [(i, (i + d) % n) for i in range(n)])]
    pallas_call x9 -> x10, Pallas kernels: 3.94 us -> 5.11 us  [call(): pl.pallas_call(kernel, out_shape=outs, in_specs=[pl.BlockSpec(memory_spac...]
    unnamed x14 -> x16, local copies, waits for them, and re-layouts: 2.8 us -> 3.78 us
  transfers between devices with their start and end apart: 2 -> 8, of which waited for: 2 -> 4; matrix products, arithmetic and copies ran while one was open for 0% -> 0% of each run, Pallas kernels for 0% -> 1%
where the time goes in v2:
time: 150 us; the launch traced here: 149 us
  blocking collectives  76.2 us (51%)
  starting transfers between devices  42.3 us (28%)
  waiting for transfers between devices  20.5 us (14%)
  Pallas kernels  6.28 us (4%)
  local copies, waits for them, and re-layouts  3.78 us (3%)
    all_to_all x5, blocking collectives, exchange(): return lax.all_to_all(value, axes, 0, 0, tiled=True)  76.2 us
    ppermute x6, starting transfers between devices, passed(): lax.ppermute(pieces[d], axis, [(i, (i + d) % n) for i in range(n)])  30.5 us
    all_to_all x2, waiting for transfers between devices, exchange(): return lax.all_to_all(value, axes, 0, 0, tiled=True)  12.1 us
    all_to_all x2, starting transfers between devices, exchange(): return lax.all_to_all(value, axes, 0, 0, tiled=True)  11.8 us
    ppermute x6, waiting for transfers between devices, passed(): lax.ppermute(pieces[d], axis, [(i, (i + d) % n) for i in range(n)])  8.4 us
    pallas_call x10, Pallas kernels, call(): pl.pallas_call(kernel, out_shape=outs, in_specs=[pl.BlockSpec(memory_spac...  5.11 us
    unnamed x16, local copies, waits for them, and re-layouts  3.78 us
  transfers between devices with their start and end apart: 8, of which 4 were waited for; matrix products, arithmetic and copies ran while one was open for 0% of the time, Pallas kernels for 1%

profile of v2, /device:TPU:2, one launch (start us, length us, event | category | flops | bytes accessed | tf_op | source)
XLA Modules:
  0.0 149.2 jit_solution(2695784843018999906)
XLA Ops:
  0.0 0.0 copy-start
  0.0 1.2 copy-done
  1.2 0.0 copy-start.1
  1.2 1.2 copy-done.1
  2.5 0.0 copy-start.3
  2.5 0.0 copy-start.5
  2.5 1.0 shard_map.85
  3.5 3.4 %collective-permute-start = (bf16[2,128,1024]{2,1,0:T(8,128)(2,1)}, bf16[2,128,1024]{2,1,0:T(8,128)(2,1)S(1)}, u32[]{:S(2)}, u32[]{:S(2)}) collective-permute-start(bf16[2,128,1024]{2,1,0:T(8,128)(2,1)} %get-tuple-element.19), channel_id=1, source_target_pairs={{0,1},{1,2},{2,3},{3,0},{4,5},{5,6},{6,7},{7,4},{8,9},{9,10},{10,1... | collective-permute-start | bytes 1572872 | tf_op jit(solution)/shard_map/ppermute | solution.py:151
  6.9 15.6 %collective-permute-start.1 = (bf16[2,128,1024]{2,1,0:T(8,128)(2,1)S(1)}, bf16[2,128,1024]{2,1,0:T(8,128)(2,1)S(1)}, u32[]{:S(2)}, u32[]{:S(2)}) collective-permute-start(bf16[2,128,1024]{2,1,0:T(8,128)(2,1)S(1)} %get-tuple-element.20), channel_id=1, source_target_pairs={{0,2},{1,3},{2,0},{3,1},{4,6},{5,7},{6,4},{7,5},{8,10},{9,11},{10,... | collective-permute-start | bytes 1572872 | tf_op jit(solution)/shard_map/ppermute | solution.py:151
  22.6 1.9 %collective-permute-start.2 = (bf16[2,128,1024]{2,1,0:T(8,128)(2,1)S(1)}, bf16[2,128,1024]{2,1,0:T(8,128)(2,1)S(1)}, u32[]{:S(2)}, u32[]{:S(2)}) collective-permute-start(bf16[2,128,1024]{2,1,0:T(8,128)(2,1)S(1)} %get-tuple-element.21), channel_id=1, source_target_pairs={{0,3},{1,0},{2,1},{3,2},{4,7},{5,4},{6,5},{7,6},{8,11},{9,8},{10,9... | collective-permute-start | bytes 1572872 | tf_op jit(solution)/shard_map/ppermute | solution.py:151
  24.5 0.0 copy-done.3
  24.5 0.0 copy-done.5
  24.5 0.9 shard_map.82
  25.4 8.4 %all-to-all-start = ((bf16[16,8,128]{2,1,0:T(8,128)(2,1)}), bf16[16,8,128]{2,1,0:T(8,128)(2,1)S(1)}, u32[]{:S(2)}, u32[]{:S(2)}) async-start(bf16[16,8,128]{2,1,0:T(8,128)(2,1)} %bitcast.2), calls=%async_computation | async-start | bytes 65536 | tf_op jit(solution)/shard_map/all_to_all | solution.py:257
  33.8 0.5 shard_map.83.sel_ref
  34.3 12.1 %all-to-all-done = bf16[16,8,128]{2,1,0:T(8,128)(2,1)S(1)} async-done(((bf16[16,8,128]{2,1,0:T(8,128)(2,1)}), bf16[16,8,128]{2,1,0:T(8,128)(2,1)S(1)}, u32[]{:S(2)}, u32[]{:S(2)}) %all-to-all-start) | async-done | bytes 32800 | tf_op jit(solution)/shard_map/all_to_all | solution.py:257
  46.4 0.0 copy-start.6
  46.4 0.7 copy-done.6
  47.1 0.2 shard_map.84
  47.2 8.4 %all_to_all.35.rows_ref = bf16[8,72,128]{2,1,0:T(8,128)(2,1)S(1)} all-to-all(bf16[8,72,128]{2,1,0:T(8,128)(2,1)S(1)} %shard_map.84), channel_id=1, replica_groups=mesh['z'=16,'c'=2,'y'=8,'x'=4] {'c','x'}, dimensions={0} | all-to-all | bytes 294912 | tf_op jit(solution)/shard_map/all_to_all | solution.py:257
  55.7 0.0 collective-permute-done.refs_1_
  55.7 0.0 collective-permute-done.1.refs_2_
  55.7 0.0 collective-permute-done.2.refs_3_
  55.7 0.7 shard_map.86
  56.4 0.0 copy-start.2
  56.4 25.5 %all_to_all.36.refs_0_ = bf16[8,16,2176]{2,1,0:T(8,128)(2,1)S(1)} all-to-all(bf16[8,16,2176]{2,1,0:T(8,128)(2,1)S(1)} %bitcast.14), channel_id=1, replica_groups=mesh['z'=16,'c'=2,'y'=8,'x'=4] {'y'}, dimensions={0} | all-to-all | bytes 1114112 | tf_op jit(solution)/shard_map/all_to_all | solution.py:257
  81.9 0.9 shard_map.87
  82.8 3.4 %all-to-all-start.3 = ((bf16[8,16,1024]{2,1,0:T(8,128)(2,1)}), bf16[8,16,1024]{2,1,0:T(8,128)(2,1)S(1)}, u32[]{:S(2)}, u32[]{:S(2)}) async-start(bf16[8,16,1024]{2,1,0:T(8,128)(2,1)} %shard_map.87), calls=%async_computation.3 | async-start | bytes 524288 | tf_op jit(solution)/shard_map/all_to_all | solution.py:257
  86.2 0.0 copy-done.2
  86.2 0.0 copy-start.4
  86.2 0.1 shard_map.89
  86.4 2.0 %collective-permute-start.3 = (bf16[1,1024,128]{2,1,0:T(8,128)(2,1)S(1)}, bf16[1,1024,128]{2,1,0:T(8,128)(2,1)S(1)}, u32[]{:S(2)}, u32[]{:S(2)}) collective-permute-start(bf16[1,1024,128]{2,1,0:T(8,128)(2,1)S(1)} %get-tuple-element.23), channel_id=1, source_target_pairs={{0,1},{1,2},{2,3},{3,0},{4,5},{5,6},{6,7},{7,4},{8,9},{9,10},{10,1... | collective-permute-start | bytes 786440 | tf_op jit(solution)/shard_map/ppermute | solution.py:151
  88.4 4.9 %collective-permute-start.4 = (bf16[1,1024,128]{2,1,0:T(8,128)(2,1)S(1)}, bf16[1,1024,128]{2,1,0:T(8,128)(2,1)S(1)}, u32[]{:S(2)}, u32[]{:S(2)}) collective-permute-start(bf16[1,1024,128]{2,1,0:T(8,128)(2,1)S(1)} %get-tuple-element.24), channel_id=1, source_target_pairs={{0,2},{1,3},{2,0},{3,1},{4,6},{5,7},{6,4},{7,5},{8,10},{9,11},{10,... | collective-permute-start | bytes 786440 | tf_op jit(solution)/shard_map/ppermute | solution.py:151
  93.4 2.6 %collective-permute-start.5 = (bf16[1,1024,128]{2,1,0:T(8,128)(2,1)S(1)}, bf16[1,1024,128]{2,1,0:T(8,128)(2,1)S(1)}, u32[]{:S(2)}, u32[]{:S(2)}) collective-permute-start(bf16[1,1024,128]{2,1,0:T(8,128)(2,1)S(1)} %get-tuple-element.25), channel_id=1, source_target_pairs={{0,3},{1,0},{2,1},{3,2},{4,7},{5,4},{6,5},{7,6},{8,11},{9,8},{10,9... | collective-permute-start | bytes 786440 | tf_op jit(solution)/shard_map/ppermute | solution.py:151
  95.9 0.0 copy-done.4
  95.9 0.3 shard_map.88.scale_ref
  96.2 1.3 collective-permute-done.3.refs_1_
  97.5 3.6 %collective-permute-done.4.refs_2_ = bf16[1,1024,128]{2,1,0:T(8,128)(2,1)S(1)} collective-permute-done((bf16[1,1024,128]{2,1,0:T(8,128)(2,1)S(1)}, bf16[1,1024,128]{2,1,0:T(8,128)(2,1)S(1)}, u32[]{:S(2)}, u32[]{:S(2)}) %collective-permute-start.4) | collective-permute-done | bytes 262176 | tf_op jit(solution)/shard_map/ppermute | solution.py:151
  101.0 3.6 %collective-permute-done.5.refs_3_ = bf16[1,1024,128]{2,1,0:T(8,128)(2,1)S(1)} collective-permute-done((bf16[1,1024,128]{2,1,0:T(8,128)(2,1)S(1)}, bf16[1,1024,128]{2,1,0:T(8,128)(2,1)S(1)}, u32[]{:S(2)}, u32[]{:S(2)}) %collective-permute-start.5) | collective-permute-done | bytes 262176 | tf_op jit(solution)/shard_map/ppermute | solution.py:151
  104.6 0.0 all-to-all-done.3
  104.6 0.4 shard_map.90
  105.0 9.6 %all_to_all.37.parts_ref = bf16[8,64,128]{2,1,0:T(8,128)(2,1)S(1)} all-to-all(bf16[8,64,128]{2,1,0:T(8,128)(2,1)S(1)} %shard_map.90), channel_id=1, replica_groups=mesh['z'=16,'c'=2,'y'=8,'x'=4] {'c','x'}, dimensions={0} | all-to-all | bytes 262144 | tf_op jit(solution)/shard_map/all_to_all | solution.py:257
  114.6 0.2 shard_map.91
  114.8 15.0 %all_to_all.38 = bf16[16,8,128]{2,1,0:T(8,128)(2,1)S(1)} all-to-all(bf16[16,8,128]{2,1,0:T(8,128)(2,1)S(1)} %bitcast.20), channel_id=1, replica_groups=mesh['z'=16,'c'=2,'y'=8,'x'=4] {'z'}, dimensions={0} | all-to-all | bytes 65536 | tf_op jit(solution)/shard_map/all_to_all | solution.py:257
  129.9 0.3 shard_map.92
  130.2 17.6 %all_to_all.39.refs_0_ = f32[32,1,128]{2,1,0:T(1,128)S(1)} all-to-all(f32[32,1,128]{2,1,0:T(1,128)S(1)} %get-tuple-element.27), channel_id=1, replica_groups=mesh['z'=16,'c'=2,'y'=8,'x'=4] {'y','x'}, dimensions={0} | all-to-all | bytes 32768 | tf_op jit(solution)/shard_map/all_to_all | solution.py:257
  147.8 0.7 copy-done.7
  148.4 0.8 shard_map.93
  (1 shorter events, 0.0 us)
Async XLA Ops:
  0.0 1.2 copy-start
  1.2 1.2 copy-start.1
  2.5 22.0 %copy-start.3 = (s32[2048,4]{0,1:T(4,128)S(1)}, s32[2048,4]{0,1:T(4,128)}, u32[]{:S(2)}) copy-start(s32[2048,4]{0,1:T(4,128)} %param.11) | copy-start | bytes 98308
  2.5 22.0 %copy-start.5 = (bf16[64,128]{1,0:T(8,128)(2,1)S(1)}, bf16[64,128]{1,0:T(8,128)(2,1)}, u32[]{:S(2)}) copy-start(bf16[64,128]{1,0:T(8,128)(2,1)} %tok_ref.1) | copy-start | bytes 49156
  3.5 52.2 %collective-permute-start = (bf16[2,128,1024]{2,1,0:T(8,128)(2,1)}, bf16[2,128,1024]{2,1,0:T(8,128)(2,1)S(1)}, u32[]{:S(2)}, u32[]{:S(2)}) collective-permute-start(bf16[2,128,1024]{2,1,0:T(8,128)(2,1)} %get-tuple-element.19), channel_id=1, source_target_pairs={{0,1},{1,2},{2,3},{3,0},{4,5},{5,6},{6,7},{7,4},{8,9},{9,10},{10,1... | collective-permute-start | bytes 1572872 | tf_op jit(solution)/shard_map/ppermute | solution.py:151
  6.9 48.8 %collective-permute-start.1 = (bf16[2,128,1024]{2,1,0:T(8,128)(2,1)S(1)}, bf16[2,128,1024]{2,1,0:T(8,128)(2,1)S(1)}, u32[]{:S(2)}, u32[]{:S(2)}) collective-permute-start(bf16[2,128,1024]{2,1,0:T(8,128)(2,1)S(1)} %get-tuple-element.20), channel_id=1, source_target_pairs={{0,2},{1,3},{2,0},{3,1},{4,6},{5,7},{6,4},{7,5},{8,10},{9,11},{10,... | collective-permute-start | bytes 1572872 | tf_op jit(solution)/shard_map/ppermute | solution.py:151
  22.6 33.1 %collective-permute-start.2 = (bf16[2,128,1024]{2,1,0:T(8,128)(2,1)S(1)}, bf16[2,128,1024]{2,1,0:T(8,128)(2,1)S(1)}, u32[]{:S(2)}, u32[]{:S(2)}) collective-permute-start(bf16[2,128,1024]{2,1,0:T(8,128)(2,1)S(1)} %get-tuple-element.21), channel_id=1, source_target_pairs={{0,3},{1,0},{2,1},{3,2},{4,7},{5,4},{6,5},{7,6},{8,11},{9,8},{10,9... | collective-permute-start | bytes 1572872 | tf_op jit(solution)/shard_map/ppermute | solution.py:151
  25.4 21.0 %all-to-all-start = ((bf16[16,8,128]{2,1,0:T(8,128)(2,1)}), bf16[16,8,128]{2,1,0:T(8,128)(2,1)S(1)}, u32[]{:S(2)}, u32[]{:S(2)}) async-start(bf16[16,8,128]{2,1,0:T(8,128)(2,1)} %bitcast.2), calls=%async_computation | async-start | bytes 65536 | tf_op jit(solution)/shard_map/all_to_all | solution.py:257
  46.4 0.7 copy-start.6
  56.4 29.8 %copy-start.2 = (bf16[4,1024,128]{2,1,0:T(8,128)(2,1)S(1)}, bf16[4,1024,128]{2,1,0:T(8,128)(2,1)}, u32[]{:S(2)}) copy-start(bf16[4,1024,128]{2,1,0:T(8,128)(2,1)} %refs_0_.3) | copy-start | bytes 3145732
  82.8 21.8 %all-to-all-start.3 = ((bf16[8,16,1024]{2,1,0:T(8,128)(2,1)}), bf16[8,16,1024]{2,1,0:T(8,128)(2,1)S(1)}, u32[]{:S(2)}, u32[]{:S(2)}) async-start(bf16[8,16,1024]{2,1,0:T(8,128)(2,1)} %shard_map.87), calls=%async_computation.3 | async-start | bytes 524288 | tf_op jit(solution)/shard_map/all_to_all | solution.py:257
  86.2 9.7 %copy-start.4 = (f32[2048,4]{0,1:T(4,128)S(1)}, f32[2048,4]{0,1:T(4,128)}, u32[]{:S(2)}) copy-start(f32[2048,4]{0,1:T(4,128)} %param.12) | copy-start | bytes 98308
  86.4 11.1 %collective-permute-start.3 = (bf16[1,1024,128]{2,1,0:T(8,128)(2,1)S(1)}, bf16[1,1024,128]{2,1,0:T(8,128)(2,1)S(1)}, u32[]{:S(2)}, u32[]{:S(2)}) collective-permute-start(bf16[1,1024,128]{2,1,0:T(8,128)(2,1)S(1)} %get-tuple-element.23), channel_id=1, source_target_pairs={{0,1},{1,2},{2,3},{3,0},{4,5},{5,6},{6,7},{7,4},{8,9},{9,10},{10,1... | collective-permute-start | bytes 786440 | tf_op jit(solution)/shard_map/ppermute | solution.py:151
  88.4 12.6 %collective-permute-start.4 = (bf16[1,1024,128]{2,1,0:T(8,128)(2,1)S(1)}, bf16[1,1024,128]{2,1,0:T(8,128)(2,1)S(1)}, u32[]{:S(2)}, u32[]{:S(2)}) collective-permute-start(bf16[1,1024,128]{2,1,0:T(8,128)(2,1)S(1)} %get-tuple-element.24), channel_id=1, source_target_pairs={{0,2},{1,3},{2,0},{3,1},{4,6},{5,7},{6,4},{7,5},{8,10},{9,11},{10,... | collective-permute-start | bytes 786440 | tf_op jit(solution)/shard_map/ppermute | solution.py:151
  93.4 11.2 %collective-permute-start.5 = (bf16[1,1024,128]{2,1,0:T(8,128)(2,1)S(1)}, bf16[1,1024,128]{2,1,0:T(8,128)(2,1)S(1)}, u32[]{:S(2)}, u32[]{:S(2)}) collective-permute-start(bf16[1,1024,128]{2,1,0:T(8,128)(2,1)S(1)} %get-tuple-element.25), channel_id=1, source_target_pairs={{0,3},{1,0},{2,1},{3,2},{4,7},{5,4},{6,5},{7,6},{8,11},{9,8},{10,9... | collective-permute-start | bytes 786440 | tf_op jit(solution)/shard_map/ppermute | solution.py:151
  147.8 0.7 copy-start.7
